TPU v7x, 32 devices: a whole 2x2x4 slice. The times are simulated.
32 devices in a mesh: sp: 8 (over z, x), tp: 4 (over y, core).
Axes of the slice: x: 2, y: 2, z: 4, core: 2. Of those that a mesh axis runs over, the one named last changes fastest.
Arguments:
- tokens: bfloat16 [2048, 2048], P('sp'), may hold values from -6 to 6
- documents: int32 [2048], P('sp'), may hold values from 0 to 3, never falling along the last dimension, each value on 1 to 1024 neighbouring positions
- norm_gain: float32 [1, 2048], replicated, may hold values from 0.1 to 1.9
- w_query: bfloat16 [1, 2048, 2048], P(None, 'sp', 'tp'), may hold values from -0.125 to 0.125
- w_key: bfloat16 [1, 2048, 2048], P(None, 'sp', 'tp'), may hold values from -0.125 to 0.125
- w_value: bfloat16 [1, 2048, 2048], P(None, 'sp', 'tp'), may hold values from -0.125 to 0.125
- w_out: bfloat16 [1, 2048, 2048], P(None, None, 'sp'), may hold values from -0.59765625 to 0.59765625
- rel_bias: float32 [1, 32, 257], P(None, 'tp'), may hold values from -8 to 240
Outputs:
- mixed: bfloat16 [2048, 2048], P('sp')
Inputs may be any that keep to these rules, and one draw needn't show every extreme that they name: `documents`: document numbers never fall along the sequence; a document has 1 to 1024 positions.
All inputs are finite; a program needn't handle non-finite values.
Results may differ from a plain program's by a relative error of at most 0.007.
Values may be sent and summed in bfloat16 or wider, within the bound.
A program may use at most 128 MiB of HBM per device.

v0:
```python
import jax
import jax.numpy as jnp
from jax import lax
from jax.sharding import PartitionSpec as P

HEAD_DIM = 64
SEG = 64
LEFT = 4
REL_CLIP = 128


EPS = 1e-06


def passed_along(x, axis, by):
    length = lax.axis_size(axis)
    pairs = [(i, i + by) for i in range(length) if 0 <= i + by < length]
    return lax.ppermute(x, axis, pairs)


def banded_bias(bias_table, query_rows, key_rows, reach_rows):
    span_len = query_rows + key_rows - 1
    steps_back = jnp.arange(span_len, dtype=jnp.int32) - (key_rows - 1) + reach_rows
    lookup = jnp.clip(steps_back, -REL_CLIP, REL_CLIP) + REL_CLIP
    bias_line = jnp.take(bias_table, lookup, axis=1)
    reversed_line = bias_line[:, ::-1]
    repeated = jnp.tile(reversed_line, (1, query_rows))
    skewed = repeated[:, query_rows - 1 : query_rows - 1 + query_rows * (span_len - 1)]
    skewed = skewed.reshape(bias_table.shape[0], query_rows, span_len - 1)
    return skewed[:, :, :key_rows]


def attend(queries, keys_all, values_all, query_pos, key_pos, query_doc, key_doc, bias_table):
    query_rows = queries.shape[0]
    key_rows = keys_all.shape[0]
    reach_rows = key_rows - query_rows
    scores = jnp.einsum(
        "qhe,khe->hqk", queries, keys_all, preferred_element_type=jnp.float32
    ) * HEAD_DIM ** (-0.5)
    scores = scores + banded_bias(bias_table, query_rows, key_rows, reach_rows)
    query_seg = query_pos // SEG
    key_seg = key_pos // SEG
    allowed = (
        (key_pos[None, :] >= 0)
        & (key_seg[None, :] <= query_seg[:, None])
        & (key_seg[None, :] >= query_seg[:, None] - LEFT)
        & (key_doc[None, :] == query_doc[:, None])
    )
    scores = jnp.where(allowed[None], scores, -1e30)
    peak = jnp.max(scores, axis=-1, keepdims=True)
    raised = jnp.exp(scores - peak)
    weights_bf = (raised / jnp.sum(raised, axis=-1, keepdims=True)).astype(jnp.bfloat16)
    return jnp.einsum(
        "hqk,khe->qhe", weights_bf, values_all, preferred_element_type=jnp.float32
    ).astype(jnp.bfloat16)


def body(tokens, documents, norm_gain, w_query, w_key, w_value, w_out, rel_bias):
    local_rows = tokens.shape[0]
    reach_rows = LEFT * SEG
    width_local = w_query.shape[2]
    heads_local = width_local // HEAD_DIM
    offset = lax.axis_index("sp") * local_rows
    query_pos = offset + jnp.arange(local_rows, dtype=jnp.int32)
    key_pos = offset - reach_rows + jnp.arange(reach_rows + local_rows, dtype=jnp.int32)
    widened = tokens.astype(jnp.float32)
    normed = (
        widened
        * lax.rsqrt(jnp.mean(widened * widened, axis=-1, keepdims=True) + EPS)
        * norm_gain[0]
    ).astype(jnp.bfloat16)
    query_sum = jnp.dot(
        normed,
        lax.all_gather(w_query[0], "sp", axis=0, tiled=True),
        preferred_element_type=jnp.float32,
    )
    key_sum = jnp.dot(
        normed,
        lax.all_gather(w_key[0], "sp", axis=0, tiled=True),
        preferred_element_type=jnp.float32,
    )
    value_sum = jnp.dot(
        normed,
        lax.all_gather(w_value[0], "sp", axis=0, tiled=True),
        preferred_element_type=jnp.float32,
    )
    queries = query_sum.astype(jnp.bfloat16)
    keys_own = key_sum.astype(jnp.bfloat16)
    values_own = value_sum.astype(jnp.bfloat16)
    prior_keys, prior_values, prior_docs = passed_along((keys_own, values_own, documents), "sp", 1)
    keys_all = jnp.concatenate([prior_keys, keys_own], axis=0)
    values_all = jnp.concatenate([prior_values, values_own], axis=0)
    key_doc = jnp.concatenate([prior_docs, documents], axis=0)
    attended = attend(
        queries.reshape(local_rows, heads_local, HEAD_DIM),
        keys_all.reshape(reach_rows + local_rows, heads_local, HEAD_DIM),
        values_all.reshape(reach_rows + local_rows, heads_local, HEAD_DIM),
        query_pos,
        key_pos,
        documents,
        key_doc,
        rel_bias[0],
    ).reshape(local_rows, width_local)
    all_heads = lax.all_gather(attended, "tp", axis=1, tiled=True)
    return (
        widened
        + jnp.dot(
            all_heads,
            lax.all_gather(w_out[0], "sp", axis=1, tiled=True),
            preferred_element_type=jnp.float32,
        )
    ).astype(jnp.bfloat16)


def solution(mesh):
    in_specs = (
        P("sp", None),
        P("sp"),
        P(),
        P(None, "sp", "tp"),
        P(None, "sp", "tp"),
        P(None, "sp", "tp"),
        P(None, None, "sp"),
        P(None, "tp", None),
    )
    out_specs = P("sp", None)
    return jax.shard_map(body, mesh=mesh, in_specs=in_specs, out_specs=out_specs, check_vma=False)
```

profile of v0, /device:TPU:0, one launch (start us, length us, event | category | flops | bytes accessed | tf_op | source)
XLA Modules:
  0.0 332.9 jit_solution(15047874739899325037)
XLA Ops:
  6.5 0.7 all-gather.12.cloned.1.call-update
  7.3 0.7 all-gather.16.cloned.1.call-update
  8.8 4.9 %collective-permute-start.1 = (s32[256]{0:T(256)}, s32[256]{0:T(256)S(1)}, u32[]{:S(2)}, u32[]{:S(2)}) collective-permute-start(s32[256]{0:T(256)} %param.9), channel_id=1, source_target_pairs={{0,4},{4,8},{8,12},{12,16},{16,20},{20,24},{24,28},{1,5},{5,9},{9,... | collective-permute-start | bytes 3080 | tf_op jit(solution)/shard_map/ppermute | solution.py:18
  13.7 0.8 copy.17
  14.6 1.6 gather_fusion
  16.2 1.5 fusion.9
  18.5 3.1 tile.4
  21.6 8.7 %tile.10 = f32[8,196352]{1,0:T(8,128)} reshape(f32[8,256,767]{2,1,0:T(8,128)} %tile.4) | data formatting | bytes 12566528 | tf_op jit(solution)/shard_map/tile | solution.py:27
  30.3 5.4 %slice.10 = f32[8,196096]{1,0:T(8,128)} slice(f32[8,196352]{1,0:T(8,128)} %tile.10), slice={[0:8], [255:196351]} | slice | bytes 12550144 | tf_op jit(solution)/shard_map/slice | solution.py:28
  35.7 12.4 %reshape.203 = f32[8,256,766]{2,1,0:T(8,128)} reshape(f32[8,196096]{1,0:T(8,128)} %slice.10) | data formatting | bytes 12550144 | tf_op jit(solution)/shard_map/reshape | solution.py:29
  48.4 12.9 %all-gather.12.cloned.1.call-done = bf16[1,2048,512]{2,1,0:T(8,128)(2,1)} async-done(((bf16[1,256,512]{2,1,0:T(8,128)(2,1)}), bf16[1,2048,512]{2,1,0:T(8,128)(2,1)}) %all-gather.12.cloned.1.call-update) | async-done | bytes 2097168 | tf_op jit(solution)/shard_map/all_gather | solution.py:84
  61.3 2.3 fusion.20
  63.7 2.5 collective-permute-start
  66.1 45.1 %all-gather.16.cloned.1.call-done = bf16[1,2048,512]{2,1,0:T(8,128)(2,1)} async-done(((bf16[1,256,512]{2,1,0:T(8,128)(2,1)}), bf16[1,2048,512]{2,1,0:T(8,128)(2,1)}) %all-gather.16.cloned.1.call-update) | async-done | bytes 2097168 | tf_op jit(solution)/shard_map/all_gather | solution.py:79
  111.2 2.3 fusion.26
  113.5 2.7 collective-permute-start.2
  116.3 44.9 %all-gather.14.cloned.1.call-done = bf16[1,2048,512]{2,1,0:T(8,128)(2,1)} async-done(((bf16[1,256,512]{2,1,0:T(8,128)(2,1)}), bf16[1,2048,512]{2,1,0:T(8,128)(2,1)}) %all-gather.14.cloned.1.call-update) | async-done | bytes 2097168 | tf_op jit(solution)/shard_map/all_gather | solution.py:74
  161.1 2.3 fusion.23
  164.1 3.1 fusion.3
  167.2 1.7 fusion.41
  169.2 8.0 %fusion.19 = bf16[8,64,256]{2,1,0:T(8,128)(2,1)} fusion(bf16[512,8,64]{0,2,1:T(8,128)(2,1)S(1)} %bitcast.41, f32[8,256]{1,0:T(8,128)S(1)} %fusion.41, f32[8,256,512]{2,1,0:T(8,128)} %copy-done), kind=kOutput, calls=%fused_computation.22 | convolution fusion | flops 137497088 | bytes 4988928 | tf_op jit(solution)/shard_map/hqk,khe->qhe/dot_general | solution.py:53
  177.7 14.8 %all-gather.10.cloned.1.call-done = bf16[256,2048]{0,1:T(8,128)(2,1)} async-done(((bf16[256,512]{0,1:T(8,128)(2,1)}), bf16[256,2048]{0,1:T(8,128)(2,1)}) %all-gather.10.cloned.1.call-update) | async-done | bytes 1048592 | tf_op jit(solution)/shard_map/all_gather | solution.py:104
  192.5 126.8 %all-gather.18.cloned.1.call-done = bf16[1,2048,2048]{2,1,0:T(8,128)(2,1)} async-done(((bf16[1,2048,256]{2,1,0:T(8,128)(2,1)}), bf16[1,2048,2048]{2,1,0:T(8,128)(2,1)}) %all-gather.18.cloned.1.call-update) | async-done | bytes 8388624 | tf_op jit(solution)/shard_map/all_gather | solution.py:109
  319.4 7.0 %fusion.6 = bf16[256,2048]{1,0:T(8,128)(2,1)} fusion(bf16[256,2048]{0,1:T(8,128)(2,1)} %all-gather.10.cloned.1.call-done, bf16[1,2048,2048]{2,1,0:T(8,128)(2,1)} %all-gather.18.cloned.1.call-done, bf16[256,2048]{1,0:T(8,128)(2,1)S(1)} %copy-done.1), kind=kOutput, calls=%fused_computation.11 | convolution fusion | flops 2149056512 | bytes 11534336 | tf_op jit(solution)/shard_map/dot_general | solution.py:107
  (36 shorter events, 3.3 us)
Async XLA Ops:
  6.5 54.8 %all-gather.12.cloned.1.call-start = ((), (), s32[]{:S(2)}) async-start(), calls=%async_computation.1 | async-start | bytes 2359296 | tf_op jit(solution)/shard_map/all_gather | solution.py:84
  7.3 103.9 %all-gather.16.cloned.1.call-start = ((), (), s32[]{:S(2)}) async-start(), calls=%async_computation.3 | async-start | bytes 2359296 | tf_op jit(solution)/shard_map/all_gather | solution.py:79
  8.0 153.1 %all-gather.14.cloned.1.call-start = ((), (), s32[]{:S(2)}) async-start(), calls=%async_computation.2 | async-start | bytes 2359296 | tf_op jit(solution)/shard_map/all_gather | solution.py:74
  8.7 183.8 %all-gather.10.cloned.1.call-start = ((), (), s32[]{:S(2)}) async-start(), calls=%async_computation | async-start | bytes 1310720 | tf_op jit(solution)/shard_map/all_gather | solution.py:104
  8.8 39.3 %collective-permute-start.1 = (s32[256]{0:T(256)}, s32[256]{0:T(256)S(1)}, u32[]{:S(2)}, u32[]{:S(2)}) collective-permute-start(s32[256]{0:T(256)} %param.9), channel_id=1, source_target_pairs={{0,4},{4,8},{8,12},{12,16},{16,20},{20,24},{24,28},{1,5},{5,9},{9,... | collective-permute-start | bytes 3080 | tf_op jit(solution)/shard_map/ppermute | solution.py:18
  35.7 12.4 %copy-start.2 = (s32[256]{0:T(256)S(1)}, s32[256]{0:T(256)}, u32[]{:S(2)}) copy-start(s32[256]{0:T(256)} %param.9) | copy-start | bytes 3076
  35.7 25.6 %copy-start.1 = (bf16[256,2048]{1,0:T(8,128)(2,1)S(1)}, bf16[256,2048]{1,0:T(8,128)(2,1)}, u32[]{:S(2)}) copy-start(bf16[256,2048]{1,0:T(8,128)(2,1)} %param.8) | copy-start | bytes 3145732
  35.7 25.6 %copy-start.3 = (f32[1,2048]{1,0:T(1,128)S(1)}, f32[1,2048]{1,0:T(1,128)}, u32[]{:S(2)}) copy-start(f32[1,2048]{1,0:T(1,128)} %param.10) | copy-start | bytes 24580
  63.7 100.0 %collective-permute-start = (bf16[256,512]{1,0:T(8,128)(2,1)S(1)}, bf16[256,512]{1,0:T(8,128)(2,1)S(1)}, u32[]{:S(2)}, u32[]{:S(2)}) collective-permute-start(bf16[256,512]{1,0:T(8,128)(2,1)S(1)} %fusion.20), channel_id=1, source_target_pairs={{0,4},{4,8},{8,12},{12,16},{16,20},{20,24},{24,28},{1,5},{5,9},{9,... | collective-permute-start | bytes 786440 | tf_op jit(solution)/shard_map/ppermute | solution.py:18
  113.5 50.3 %collective-permute-start.2 = (bf16[256,512]{1,0:T(8,128)(2,1)S(1)}, bf16[256,512]{1,0:T(8,128)(2,1)S(1)}, u32[]{:S(2)}, u32[]{:S(2)}) collective-permute-start(bf16[256,512]{1,0:T(8,128)(2,1)S(1)} %fusion.26), channel_id=1, source_target_pairs={{0,4},{4,8},{8,12},{12,16},{16,20},{20,24},{24,28},{1,5},{5,9},{9,... | collective-permute-start | bytes 786440 | tf_op jit(solution)/shard_map/ppermute | solution.py:18
  167.2 1.9 copy-start
  177.1 142.2 %all-gather.18.cloned.1.call-start = ((), (), s32[]{:S(2)}) async-start(), calls=%async_computation.4 | async-start | bytes 9437184 | tf_op jit(solution)/shard_map/all_gather | solution.py:109
Sparse Core Ops, SparseCore 0:
  9.5 51.7 all-gather.11
  63.4 47.7 all-gather.15
  113.3 47.7 all-gather.13
  177.3 15.2 all-gather.9
  194.4 124.9 all-gather.17
where the time goes:
time: 333 us
  waiting for transfers between devices  247 us (74%)
  local copies, waits for them, and re-layouts  33.3 us (10%)
  matrix products  25.1 us (8%)
  between operations  13.3 us (4%)
  starting transfers between devices  10.2 us (3%)
  other arithmetic  3.84 us (1%)
    all_gather x1, waiting for transfers between devices, body(): lax.all_gather(w_out[0], 'sp', axis=1, tiled=True)  127 us
    all_gather x1, waiting for transfers between devices, body(): lax.all_gather(w_key[0], 'sp', axis=0, tiled=True)  45.1 us
    all_gather x1, waiting for transfers between devices, body(): lax.all_gather(w_query[0], 'sp', axis=0, tiled=True)  44.9 us
    all_gather x1, waiting for transfers between devices, body(): all_heads = lax.all_gather(attended, 'tp', axis=1, tiled=True)  14.8 us
    all_gather x1, waiting for transfers between devices, body(): lax.all_gather(w_value[0], 'sp', axis=0, tiled=True)  12.9 us
    reshape x1, local copies, waits for them, and re-layouts, banded_bias(): skewed = skewed.reshape(bias_table.shape[0], query_rows, span_len - 1)  12.4 us
    another operation x2, local copies, waits for them, and re-layouts, banded_bias(): repeated = jnp.tile(reversed_line, (1, query_rows))  11.8 us
    ppermute x3, starting transfers between devices, passed_along(): return lax.ppermute(x, axis, pairs)  10 us
  transfers between devices with their start and end apart: 8, of which 5 were waited for; matrix products, arithmetic and copies ran while one was open for 13% of the time, Pallas kernels for 0%

commit v1 on v0

--- a/solution.py
+++ b/solution.py
@@ -1,6 +1,10 @@
+import functools
+
 import jax
 import jax.numpy as jnp
 from jax import lax
+from jax.experimental import pallas as pl
+from jax.experimental.pallas import tpu as pltpu
 from jax.sharding import PartitionSpec as P
 
 HEAD_DIM = 64
@@ -112,7 +116,312 @@
     ).astype(jnp.bfloat16)
 
 
+MESH = pl.DeviceIdType.MESH
+KEY, VALUE, QUERY, OUT = range(4)
+UP, DOWN, ACROSS = range(3)
+NEG = -1e30
+
+
+def layer_kernel(
+    n_sp, n_tp, x_ref, doc_col, doc_row, gain_ref, line_ref, wk_in, wv_in, wq_in, wo_in, out_ref,
+    w_all, wo_all, normed, bias, q_buf, k_all, v_all, docs_all, att, part_out, part_in, hop_out, hop_in, done,
+    own_sem, send_sem, recv_sem, halo_send, halo_recv, tp_send, tp_recv, store_sem,
+):
+    rows, width = x_ref.shape
+    depth, cols = wk_in.shape
+    chunk = width // n_tp
+    lanes = 2 * HEAD_DIM
+    nz = n_sp // 2
+    s = lax.axis_index("sp")
+    t = lax.axis_index("tp")
+    z, x = s // 2, s % 2
+    mate = s + 1 - 2 * x
+    ty, tc = t // 2, t % 2
+    t_core = t + 1 - 2 * tc
+    t_y = (1 - ty) * 2 + tc
+    own_in = (wk_in, wv_in, wq_in)
+
+    def slot(kind, block):
+        if kind == OUT:
+            return wo_all.at[block]
+        return w_all.at[kind, pl.ds(pl.multiple_of(block * depth, depth), depth), :]
+
+    def own_copy(kind):
+        if kind == OUT:
+            src = wo_in.at[pl.ds(pl.multiple_of(t * cols, cols), cols), :]
+        else:
+            src = own_in[kind]
+        return pltpu.make_async_copy(src, slot(kind, s), own_sem.at[kind])
+
+    for kind in range(4):
+        own_copy(kind).start()
+
+    def move(way, kind, block):
+        target = (s + 2, s - 2, mate)[way]
+        return pltpu.make_async_remote_copy(
+            src_ref=slot(kind, block), dst_ref=slot(kind, block),
+            send_sem=send_sem.at[way, kind, block], recv_sem=recv_sem.at[kind, block],
+            device_id={"sp": target}, device_id_type=MESH,
+        )
+
+    def halo(i):
+        buf = (k_all, v_all, docs_all)[i]
+        if i == 2:
+            src, dst = buf.at[:, pl.ds(rows, rows)], buf.at[:, pl.ds(0, rows)]
+        else:
+            src, dst = buf.at[pl.ds(rows, rows), :], buf.at[pl.ds(0, rows), :]
+        return pltpu.make_async_remote_copy(
+            src_ref=src, dst_ref=dst, send_sem=halo_send.at[i], recv_sem=halo_recv.at[i],
+            device_id={"sp": s + 1}, device_id_type=MESH,
+        )
+
+    has_up, has_down = z < nz - 1, z > 0
+    has_next, has_prior = s < n_sp - 1, s > 0
+
+    barrier = pltpu.get_barrier_semaphore()
+    for by in (1, 2, n_sp - 2, n_sp - 1):
+        pl.semaphore_signal(barrier, inc=1, device_id={"sp": lax.rem(s + by, n_sp)}, device_id_type=MESH)
+    for by in range(1, n_tp):
+        pl.semaphore_signal(barrier, inc=1, device_id={"tp": lax.rem(t + by, n_tp)}, device_id_type=MESH)
+    pl.semaphore_wait(barrier, 4 + n_tp - 1)
+
+    def send_own(kind):
+        own_copy(kind).wait()
+        pl.when(has_up)(lambda: move(UP, kind, s).start())
+        pl.when(has_down)(lambda: move(DOWN, kind, s).start())
+        move(ACROSS, kind, s).start()
+
+    def forward(kind):
+        for d in range(1, nz):
+            @pl.when(z - d >= 0)
+            def _():
+                block = s - 2 * d
+                move(UP, kind, block).wait_recv()
+                pl.when(has_up)(lambda: move(UP, kind, block).start())
+                move(ACROSS, kind, block).start()
+
+            @pl.when(z + d < nz)
+            def _():
+                block = s + 2 * d
+                move(DOWN, kind, block).wait_recv()
+                pl.when(has_down)(lambda: move(DOWN, kind, block).start())
+                move(ACROSS, kind, block).start()
+
+    def arrived_across(kind):
+        for d in range(nz):
+            move(ACROSS, kind, 2 * d + 1 - x).wait_recv()
+
+    send_own(KEY)
+    send_own(VALUE)
+
+    docs_all[:, pl.ds(rows, rows)] = doc_row[...]
+    wide = x_ref[...].astype(jnp.float32)
+    normed[...] = (
+        wide * lax.rsqrt(jnp.mean(wide * wide, axis=-1, keepdims=True) + EPS) * gain_ref[...]
+    ).astype(jnp.bfloat16)
+
+    @pl.when(s == 0)
+    def _():
+        docs_all[:, pl.ds(0, rows)] = jnp.full((8, rows), -1, jnp.int32)
+        k_all[pl.ds(0, rows), :] = jnp.zeros((rows, cols), jnp.bfloat16)
+        v_all[pl.ds(0, rows), :] = jnp.zeros((rows, cols), jnp.bfloat16)
+
+    q_rows, span = 2 * SEG, (LEFT + 2) * SEG
+    q_seg = lax.broadcasted_iota(jnp.int32, (q_rows, span), 0) // SEG
+    k_seg = lax.broadcasted_iota(jnp.int32, (q_rows, span), 1) // SEG
+    near = (k_seg >= q_seg) & (k_seg <= q_seg + LEFT)
+    for h in range(cols // HEAD_DIM):
+        line = jnp.broadcast_to(line_ref[pl.ds(h, 1), :], (q_rows, line_ref.shape[1]))
+        skew = pltpu.roll(line, 0, 1, stride=1, stride_axis=0)
+        bias[h] = jnp.where(near, skew[:, :span], NEG)
+
+    pl.when(has_next)(lambda: halo(2).start())
+
+    def project(kind):
+        return jnp.dot(normed[...], w_all[kind], preferred_element_type=jnp.float32)
+
+    forward(KEY)
+    send_own(QUERY)
+    forward(VALUE)
+    arrived_across(KEY)
+    k_all[pl.ds(rows, rows), :] = project(KEY).astype(jnp.bfloat16)
+    forward(QUERY)
+    pl.when(has_next)(lambda: halo(0).start())
+    send_own(OUT)
+    arrived_across(VALUE)
+    v_all[pl.ds(rows, rows), :] = project(VALUE).astype(jnp.bfloat16)
+    forward(OUT)
+    pl.when(has_next)(lambda: halo(1).start())
+    arrived_across(QUERY)
+    q_buf[...] = (project(QUERY).astype(jnp.bfloat16).astype(jnp.float32) * HEAD_DIM ** (-0.5)).astype(jnp.bfloat16)
+
+    @pl.when(has_prior)
+    def _():
+        for i in range(3):
+            halo(i).wait_recv()
+
+    low = lax.broadcasted_iota(jnp.int32, (q_rows, lanes), 1) < HEAD_DIM
+    for j in range(rows // q_rows):
+        same = doc_col[pl.ds(j * q_rows, q_rows), :][:, :1] == docs_all[pl.ds(0, 1), pl.ds(j * q_rows, span)]
+        for p in range(cols // lanes):
+            q_pair = q_buf[pl.ds(j * q_rows, q_rows), pl.ds(p * lanes, lanes)]
+            k_pair = k_all[pl.ds(j * q_rows, span), pl.ds(p * lanes, lanes)]
+            v_pair = v_all[pl.ds(j * q_rows, span), pl.ds(p * lanes, lanes)]
+            both = []
+            for half in range(2):
+                mine = low if half == 0 else jnp.logical_not(low)
+                q_one = jnp.where(mine, q_pair, jnp.zeros_like(q_pair))
+                score = lax.dot_general(
+                    q_one, k_pair, (((1,), (1,)), ((), ())), preferred_element_type=jnp.float32
+                )
+                score = jnp.where(same, score + bias[2 * p + half], NEG)
+                raised = jnp.exp(score - jnp.max(score, axis=-1, keepdims=True))
+                total = jnp.sum(raised, axis=-1, keepdims=True)
+                both.append(
+                    jnp.dot(raised.astype(jnp.bfloat16), v_pair, preferred_element_type=jnp.float32) / total
+                )
+            att[pl.ds(j * q_rows, q_rows), pl.ds(p * lanes, lanes)] = jnp.where(low, both[0], both[1]).astype(jnp.bfloat16)
+
+    arrived_across(OUT)
+
+    def product(block):
+        return jnp.dot(att[...], wo_all[block], preferred_element_type=jnp.float32)
+
+    def chunk_product(which):
+        each = chunk // wo_in.shape[1]
+        return jnp.concatenate([product(which * each + i) for i in range(each)], axis=1)
+
+    def tp_move(i, src, dst, target):
+        return pltpu.make_async_remote_copy(
+            src_ref=src, dst_ref=dst, send_sem=tp_send.at[i], recv_sem=tp_recv.at[i],
+            device_id={"tp": target}, device_id_type=MESH,
+        )
+
+    part_moves = [tp_move(i, part_out.at[i], part_in.at[i], t_core) for i in range(2)]
+    for i in range(2):
+        other = (1 - ty if i == 0 else ty) * 2 + (1 - tc)
+        part_out[i] = chunk_product(other).astype(jnp.bfloat16)
+        part_moves[i].start()
+    far = chunk_product(t_y)
+    part_moves[0].wait_recv()
+    hop_out[...] = (far + part_in[0].astype(jnp.float32)).astype(jnp.bfloat16)
+    hop = tp_move(2, hop_out, hop_in, t_y)
+    hop.start()
+    near_sum = chunk_product(t)
+    part_moves[1].wait_recv()
+    near_sum = near_sum + part_in[1].astype(jnp.float32)
+    near_sum = near_sum + x_ref[:, pl.ds(pl.multiple_of(t * chunk, chunk), chunk)].astype(jnp.float32)
+    hop.wait_recv()
+    done[t] = (near_sum + hop_in[...].astype(jnp.float32)).astype(jnp.bfloat16)
+
+    def store(which):
+        return pltpu.make_async_copy(
+            done.at[which], out_ref.at[:, pl.ds(pl.multiple_of(which * chunk, chunk), chunk)], store_sem.at[which]
+        )
+
+    far_core = (1 - ty) * 2 + (1 - tc)
+    to_y = tp_move(3, done.at[t], done.at[t], t_y)
+    to_core = tp_move(4, done.at[t], done.at[t], t_core)
+    pass_on = tp_move(5, done.at[t_y], done.at[t_y], t_core)
+    to_y.start()
+    to_core.start()
+    store(t).start()
+    to_y.wait_recv()
+    pass_on.start()
+    store(t_y).start()
+    to_core.wait_recv()
+    store(t_core).start()
+    pass_on.wait_recv()
+    store(far_core).start()
+    for which in range(n_tp):
+        store(which).wait()
+
+    for kind in range(4):
+        for d in range(nz):
+            @pl.when(z - d >= 0)
+            def _():
+                pl.when(has_up)(lambda: move(UP, kind, s - 2 * d).wait_send())
+                move(ACROSS, kind, s - 2 * d).wait_send()
+
+            @pl.when(z + d < nz)
+            def _():
+                pl.when(has_down)(lambda: move(DOWN, kind, s + 2 * d).wait_send())
+                if d:
+                    move(ACROSS, kind, s + 2 * d).wait_send()
+    @pl.when(has_next)
+    def _():
+        for i in range(3):
+            halo(i).wait_send()
+    for one in (*part_moves, hop, to_y, to_core, pass_on):
+        one.wait_send()
+
+
+def body_one(n_sp, n_tp, tokens, documents, norm_gain, w_query, w_key, w_value, w_out, rel_bias):
+    rows, width = tokens.shape
+    depth, cols = w_query.shape[1:]
+    heads = cols // HEAD_DIM
+    out_cols = w_out.shape[2]
+    chunk = width // n_tp
+    reach = LEFT * SEG
+    table = rel_bias[0]
+    furthest = table[:, 2 * REL_CLIP:]
+    ahead, behind = reach - REL_CLIP, reach - REL_CLIP - 1
+    line = jnp.concatenate(
+        [
+            jnp.broadcast_to(furthest, (heads, ahead)),
+            table[:, ::-1],
+            jnp.broadcast_to(furthest, (heads, behind)),
+        ],
+        axis=1,
+    )
+    doc_col = jnp.broadcast_to(documents[:, None], (rows, 128))
+    doc_row = jnp.broadcast_to(documents[None, :], (8, rows))
+    bf, f32 = jnp.bfloat16, jnp.float32
+    vmem = pl.BlockSpec(memory_space=pltpu.VMEM)
+    hbm = pl.BlockSpec(memory_space=pl.ANY)
+    dma = pltpu.SemaphoreType.DMA
+    return pl.pallas_call(
+        functools.partial(layer_kernel, n_sp, n_tp),
+        out_shape=jax.ShapeDtypeStruct((rows, width), bf),
+        in_specs=[vmem] * 5 + [hbm] * 4,
+        out_specs=hbm,
+        scratch_shapes=[
+            pltpu.VMEM((3, n_sp * depth, cols), bf),
+            pltpu.VMEM((n_sp, cols, out_cols), bf),
+            pltpu.VMEM((rows, width), bf),
+            pltpu.VMEM((heads, 2 * SEG, (LEFT + 2) * SEG), f32),
+            pltpu.VMEM((rows, cols), bf),
+            pltpu.VMEM((2 * rows, cols), bf),
+            pltpu.VMEM((2 * rows, cols), bf),
+            pltpu.VMEM((8, 2 * rows), jnp.int32),
+            pltpu.VMEM((rows, cols), bf),
+            pltpu.VMEM((2, rows, chunk), bf),
+            pltpu.VMEM((2, rows, chunk), bf),
+            pltpu.VMEM((rows, chunk), bf),
+            pltpu.VMEM((rows, chunk), bf),
+            pltpu.VMEM((n_tp, rows, chunk), bf),
+            dma((4,)),
+            dma((3, 4, n_sp)),
+            dma((4, n_sp)),
+            dma((3,)),
+            dma((3,)),
+            dma((6,)),
+            dma((6,)),
+            dma((n_tp,)),
+        ],
+        compiler_params=pltpu.CompilerParams(
+            collective_id=0, has_side_effects=True, vmem_limit_bytes=48 * 1024 * 1024
+        ),
+    )(tokens, doc_col, doc_row, norm_gain, line, w_key[0], w_value[0], w_query[0], w_out[0])
+
+
+def fits_one(mesh):
+    return mesh.shape["sp"] % 2 == 0 and mesh.shape["sp"] <= 8 and mesh.shape["tp"] == 4
+
+
 def solution(mesh):
+    n_sp, n_tp = mesh.shape["sp"], mesh.shape["tp"]
+    run = functools.partial(body_one, n_sp, n_tp) if fits_one(mesh) else body
     in_specs = (
         P("sp", None),
         P("sp"),
@@ -124,4 +433,4 @@
         P(None, "tp", None),
     )
     out_specs = P("sp", None)
-    return jax.shard_map(body, mesh=mesh, in_specs=in_specs, out_specs=out_specs, check_vma=False)
+    return jax.shard_map(run, mesh=mesh, in_specs=in_specs, out_specs=out_specs, check_vma=False)

time: 333 us -> 141 us (0.42)
  the two profiles are of different devices: /device:TPU:0 before, /device:TPU:3 now
where the time goes in v1:
time: 141 us
  Pallas kernels  132 us (94%)
  local copies, waits for them, and re-layouts  8.88 us (6%)
    pallas_call x1, Pallas kernels, body_one(): pl.pallas_call(functools.partial(layer_kernel, n_sp, n_tp), out_shape=jax...  132 us
    unnamed x19, local copies, waits for them, and re-layouts  7.78 us

profile of v1, /device:TPU:3, one launch (start us, length us, event | category | flops | bytes accessed | tf_op | source)
XLA Modules:
  0.0 140.6 jit_solution(15632702481980187401)
XLA Ops:
  0.0 0.0 copy-start.6
  0.0 0.9 slice_reduce_fusion
  0.9 0.1 broadcast_in_dim.28
  0.9 0.0 copy-start.7
  0.9 0.1 broadcast_in_dim.13
  1.0 0.6 copy-done.7
  1.6 0.0 copy-done.6
  1.6 0.2 reverse
  1.9 0.1 slice.6
  1.9 0.1 pad_maximum_fusion.line_ref
  2.0 0.0 copy-start.5
  2.0 0.1 broadcast_in_dim.10.doc_col
  2.1 0.6 copy-done.5
  2.7 0.0 copy-start
  2.7 1.2 copy-done
  3.9 1.2 copy-done.1
  5.2 0.0 copy-start.2
  5.2 0.9 copy-done.2
  6.1 0.0 copy-start.3
  6.1 0.9 copy-done.3
  7.1 0.0 copy-start.4
  7.1 0.9 copy-done.4
  8.0 131.6 %shard_map.82 = bf16[256,2048]{1,0:T(8,128)(2,1)S(1)} custom-call(bf16[256,2048]{1,0:T(8,128)(2,1)S(1)} %copy-done, s32[256,128]{1,0:T(8,128)S(1)} %broadcast_in_dim.10.doc_col, s32[8,256]{1,0:T(8,128)S(1)} %broadcast_in_dim.11.doc_row, f32[1,2048]{1,0:T(1,128)S(1)} %copy-done.5, f32[8,512]{1,0:T(8,128)S(1)} %pad_maximum_fusion.line_ref, ...), custom_call_target="tpu_custom_call" | custom-call | tf_op jit(solution)/shard_map/pallas_call | solution.py:383
  139.6 1.0 copy.10
  (2 shorter events, 0.0 us)
Async XLA Ops:
  0.0 1.6 %copy-start.6 = (f32[1,8,257]{2,1,0:T(8,128)S(1)}, f32[1,8,257]{2,1,0:T(8,128)}, u32[]{:S(2)}) copy-start(f32[1,8,257]{2,1,0:T(8,128)} %param.15) | copy-start | bytes 24676
  0.9 0.7 copy-start.7
  2.0 0.7 copy-start.5
  2.7 1.2 copy-start
  3.9 1.2 copy-start.1
  5.2 0.9 copy-start.2
  6.1 0.9 copy-start.3
  7.1 0.9 copy-start.4

commit v2 on v1

--- a/solution.py
+++ b/solution.py
@@ -123,12 +123,15 @@
 
 
 def layer_kernel(
-    n_sp, n_tp, x_ref, doc_col, doc_row, gain_ref, line_ref, wk_in, wv_in, wq_in, wo_in, out_ref,
-    w_all, wo_all, normed, bias, q_buf, k_all, v_all, docs_all, att, part_out, part_in, hop_out, hop_in, done,
-    own_sem, send_sem, recv_sem, halo_send, halo_recv, tp_send, tp_recv, store_sem,
+    n_sp, n_tp, doc_col, doc_row, gain_ref, line_ref, x_in, wk_in, wv_in, wq_in, wo_in, out_ref,
+    w_all, w_mate, wo_all, x_ref, x_mate, normed, bias, q_buf, k_all, v_all, docs_all, docs_col, att, att_mate,
+    part_out, part_in, hop_out, hop_in, done,
+    own_sem, mate_sem, x_sem, send_sem, recv_sem, swap_send, swap_recv, halo_send, halo_recv,
+    tp_send, tp_recv, store_sem,
 ):
     rows, width = x_ref.shape
     depth, cols = wk_in.shape
+    half_cols = cols // 2
     chunk = width // n_tp
     lanes = 2 * HEAD_DIM
     nz = n_sp // 2
@@ -146,20 +149,33 @@
             return wo_all.at[block]
         return w_all.at[kind, pl.ds(pl.multiple_of(block * depth, depth), depth), :]
 
+    def column_half(kind, which):
+        return own_in[kind].at[:, pl.ds(pl.multiple_of(which * half_cols, half_cols), half_cols)]
+
     def own_copy(kind):
         if kind == OUT:
             src = wo_in.at[pl.ds(pl.multiple_of(t * cols, cols), cols), :]
         else:
-            src = own_in[kind]
+            src = column_half(kind, x)
         return pltpu.make_async_copy(src, slot(kind, s), own_sem.at[kind])
 
-    for kind in range(4):
+    def mate_copy(kind):
+        return pltpu.make_async_copy(column_half(kind, 1 - x), w_mate.at[kind], mate_sem.at[kind])
+
+    x_copy = pltpu.make_async_copy(x_in, x_ref, x_sem)
+    for kind in range(3):
         own_copy(kind).start()
+        mate_copy(kind).start()
+    x_copy.start()
+    own_copy(OUT).start()
 
     def move(way, kind, block):
         target = (s + 2, s - 2, mate)[way]
+        src = slot(kind, block)
+        if way == ACROSS and kind != OUT:
+            src = w_mate.at[kind]
         return pltpu.make_async_remote_copy(
-            src_ref=slot(kind, block), dst_ref=slot(kind, block),
+            src_ref=src, dst_ref=slot(kind, block),
             send_sem=send_sem.at[way, kind, block], recv_sem=recv_sem.at[kind, block],
             device_id={"sp": target}, device_id_type=MESH,
         )
@@ -167,106 +183,159 @@
     def halo(i):
         buf = (k_all, v_all, docs_all)[i]
         if i == 2:
-            src, dst = buf.at[:, pl.ds(rows, rows)], buf.at[:, pl.ds(0, rows)]
+            src, dst = buf.at[:, pl.ds(2 * rows, rows)], buf.at[:, pl.ds(0, rows)]
         else:
-            src, dst = buf.at[pl.ds(rows, rows), :], buf.at[pl.ds(0, rows), :]
+            src, dst = buf.at[pl.ds(2 * rows, rows), :], buf.at[pl.ds(0, rows), :]
         return pltpu.make_async_remote_copy(
             src_ref=src, dst_ref=dst, send_sem=halo_send.at[i], recv_sem=halo_recv.at[i],
-            device_id={"sp": s + 1}, device_id_type=MESH,
+            device_id={"sp": s + 2}, device_id_type=MESH,
         )
 
+    def block_of(which):
+        return pl.ds(pl.multiple_of(which * rows, rows), rows)
+
+    def swap(i, src, dst):
+        return pltpu.make_async_remote_copy(
+            src_ref=src, dst_ref=dst, send_sem=swap_send.at[i], recv_sem=swap_recv.at[i],
+            device_id={"sp": mate}, device_id_type=MESH,
+        )
+
+    x_swap = swap(0, x_ref, x_mate)
+    row_swap = swap(1, doc_row, docs_all.at[:, block_of(1 + x)])
+    col_swap = swap(2, doc_col, docs_col.at[block_of(x), :])
+    att_half = pl.ds(pl.multiple_of(x * half_cols, half_cols), half_cols)
+    att_swap = swap(3, att_mate, att.at[:, att_half])
+
     has_up, has_down = z < nz - 1, z > 0
-    has_next, has_prior = s < n_sp - 1, s > 0
 
     barrier = pltpu.get_barrier_semaphore()
-    for by in (1, 2, n_sp - 2, n_sp - 1):
-        pl.semaphore_signal(barrier, inc=1, device_id={"sp": lax.rem(s + by, n_sp)}, device_id_type=MESH)
-    for by in range(1, n_tp):
-        pl.semaphore_signal(barrier, inc=1, device_id={"tp": lax.rem(t + by, n_tp)}, device_id_type=MESH)
-    pl.semaphore_wait(barrier, 4 + n_tp - 1)
+    for peer in (mate, lax.rem(s + 2, n_sp), lax.rem(s + n_sp - 2, n_sp)):
+        pl.semaphore_signal(barrier, inc=1, device_id={"sp": peer}, device_id_type=MESH)
+    for peer in (t_core, t_y):
+        pl.semaphore_signal(barrier, inc=1, device_id={"tp": peer}, device_id_type=MESH)
+    pl.semaphore_wait(barrier, 5)
+
+    def along_z(kind, block):
+        pl.when(has_up)(lambda: move(UP, kind, block).start())
+        pl.when(has_down)(lambda: move(DOWN, kind, block).start())
 
     def send_own(kind):
         own_copy(kind).wait()
-        pl.when(has_up)(lambda: move(UP, kind, s).start())
-        pl.when(has_down)(lambda: move(DOWN, kind, s).start())
+        along_z(kind, s)
+        if kind == OUT:
+            move(ACROSS, kind, s).start()
+
+    def send_mate(kind):
+        mate_copy(kind).wait()
         move(ACROSS, kind, s).start()
 
-    def forward(kind):
-        for d in range(1, nz):
+    def forward_mate(kind):
+        move(ACROSS, kind, mate).wait_recv()
+        along_z(kind, mate)
+
+    def columns(kind):
+        return (s,) if kind == OUT else (s, mate)
+
+    def forward(kind, d):
+        for start in columns(kind):
             @pl.when(z - d >= 0)
             def _():
-                block = s - 2 * d
+                block = start - 2 * d
                 move(UP, kind, block).wait_recv()
                 pl.when(has_up)(lambda: move(UP, kind, block).start())
-                move(ACROSS, kind, block).start()
+                if kind == OUT:
+                    move(ACROSS, kind, block).start()
 
             @pl.when(z + d < nz)
             def _():
-                block = s + 2 * d
+                block = start + 2 * d
                 move(DOWN, kind, block).wait_recv()
                 pl.when(has_down)(lambda: move(DOWN, kind, block).start())
-                move(ACROSS, kind, block).start()
-
-    def arrived_across(kind):
-        for d in range(nz):
-            move(ACROSS, kind, 2 * d + 1 - x).wait_recv()
-
+                if kind == OUT:
+                    move(ACROSS, kind, block).start()
+
+    def normalize(src, which):
+        wide = src[...].astype(jnp.float32)
+        normed[block_of(which), :] = (
+            wide * lax.rsqrt(jnp.mean(wide * wide, axis=-1, keepdims=True) + EPS) * gain_ref[...]
+        ).astype(jnp.bfloat16)
+
+    send_mate(KEY)
     send_own(KEY)
+    send_mate(VALUE)
     send_own(VALUE)
-
-    docs_all[:, pl.ds(rows, rows)] = doc_row[...]
-    wide = x_ref[...].astype(jnp.float32)
-    normed[...] = (
-        wide * lax.rsqrt(jnp.mean(wide * wide, axis=-1, keepdims=True) + EPS) * gain_ref[...]
-    ).astype(jnp.bfloat16)
-
-    @pl.when(s == 0)
+    send_mate(QUERY)
+    x_copy.wait()
+    x_swap.start()
+    row_swap.start()
+    col_swap.start()
+
+    docs_all[:, block_of(1 + x)] = doc_row[...]
+    docs_col[block_of(x), :] = doc_col[...]
+
+    @pl.when(z == 0)
     def _():
         docs_all[:, pl.ds(0, rows)] = jnp.full((8, rows), -1, jnp.int32)
-        k_all[pl.ds(0, rows), :] = jnp.zeros((rows, cols), jnp.bfloat16)
-        v_all[pl.ds(0, rows), :] = jnp.zeros((rows, cols), jnp.bfloat16)
+        k_all[pl.ds(0, rows), :] = jnp.zeros((rows, half_cols), jnp.bfloat16)
+        v_all[pl.ds(0, rows), :] = jnp.zeros((rows, half_cols), jnp.bfloat16)
+
+    forward_mate(KEY)
+    normalize(x_ref, x)
+    forward(KEY, 1)
 
     q_rows, span = 2 * SEG, (LEFT + 2) * SEG
+    heads = half_cols // HEAD_DIM
     q_seg = lax.broadcasted_iota(jnp.int32, (q_rows, span), 0) // SEG
     k_seg = lax.broadcasted_iota(jnp.int32, (q_rows, span), 1) // SEG
     near = (k_seg >= q_seg) & (k_seg <= q_seg + LEFT)
-    for h in range(cols // HEAD_DIM):
-        line = jnp.broadcast_to(line_ref[pl.ds(h, 1), :], (q_rows, line_ref.shape[1]))
+    for h in range(heads):
+        line = jnp.broadcast_to(line_ref[pl.ds(x * heads + h, 1), :], (q_rows, line_ref.shape[1]))
         skew = pltpu.roll(line, 0, 1, stride=1, stride_axis=0)
         bias[h] = jnp.where(near, skew[:, :span], NEG)
 
-    pl.when(has_next)(lambda: halo(2).start())
-
     def project(kind):
         return jnp.dot(normed[...], w_all[kind], preferred_element_type=jnp.float32)
 
-    forward(KEY)
+    forward_mate(VALUE)
+    for d in range(2, nz):
+        forward(KEY, d)
     send_own(QUERY)
-    forward(VALUE)
-    arrived_across(KEY)
-    k_all[pl.ds(rows, rows), :] = project(KEY).astype(jnp.bfloat16)
-    forward(QUERY)
-    pl.when(has_next)(lambda: halo(0).start())
+    forward_mate(QUERY)
+    forward(VALUE, 1)
+    x_swap.wait_recv()
+    normalize(x_mate, 1 - x)
+    for d in range(2, nz):
+        forward(VALUE, d)
+    k_all[pl.ds(rows, 2 * rows), :] = project(KEY).astype(jnp.bfloat16)
+    row_swap.wait_recv()
+    col_swap.wait_recv()
+    forward(QUERY, 1)
+    pl.when(has_up)(lambda: halo(0).start())
+    pl.when(has_up)(lambda: halo(2).start())
+    v_all[pl.ds(rows, 2 * rows), :] = project(VALUE).astype(jnp.bfloat16)
+    for d in range(2, nz - 1):
+        forward(QUERY, d)
+    pl.when(has_up)(lambda: halo(1).start())
     send_own(OUT)
-    arrived_across(VALUE)
-    v_all[pl.ds(rows, rows), :] = project(VALUE).astype(jnp.bfloat16)
-    forward(OUT)
-    pl.when(has_next)(lambda: halo(1).start())
-    arrived_across(QUERY)
+    forward(QUERY, nz - 1)
     q_buf[...] = (project(QUERY).astype(jnp.bfloat16).astype(jnp.float32) * HEAD_DIM ** (-0.5)).astype(jnp.bfloat16)
 
-    @pl.when(has_prior)
+    @pl.when(has_down)
     def _():
         for i in range(3):
             halo(i).wait_recv()
 
     low = lax.broadcasted_iota(jnp.int32, (q_rows, lanes), 1) < HEAD_DIM
-    for j in range(rows // q_rows):
-        same = doc_col[pl.ds(j * q_rows, q_rows), :][:, :1] == docs_all[pl.ds(0, 1), pl.ds(j * q_rows, span)]
-        for p in range(cols // lanes):
-            q_pair = q_buf[pl.ds(j * q_rows, q_rows), pl.ds(p * lanes, lanes)]
-            k_pair = k_all[pl.ds(j * q_rows, span), pl.ds(p * lanes, lanes)]
-            v_pair = v_all[pl.ds(j * q_rows, span), pl.ds(p * lanes, lanes)]
+
+    def attend_rows(which, j):
+        first = pl.multiple_of(which * rows + j * q_rows, q_rows)
+        queries, keys = pl.ds(first, q_rows), pl.ds(first, span)
+        same = docs_col[queries, :][:, :1] == docs_all[pl.ds(0, 1), keys]
+        found = []
+        for p in range(half_cols // lanes):
+            q_pair = q_buf[queries, pl.ds(p * lanes, lanes)]
+            k_pair = k_all[keys, pl.ds(p * lanes, lanes)]
+            v_pair = v_all[keys, pl.ds(p * lanes, lanes)]
             both = []
             for half in range(2):
                 mine = low if half == 0 else jnp.logical_not(low)
@@ -280,9 +349,23 @@
                 both.append(
                     jnp.dot(raised.astype(jnp.bfloat16), v_pair, preferred_element_type=jnp.float32) / total
                 )
-            att[pl.ds(j * q_rows, q_rows), pl.ds(p * lanes, lanes)] = jnp.where(low, both[0], both[1]).astype(jnp.bfloat16)
-
-    arrived_across(OUT)
+            found.append(jnp.where(low, both[0], both[1]).astype(jnp.bfloat16))
+        return jnp.concatenate(found, axis=1)
+
+    parts = rows // q_rows
+    for j in range(parts):
+        att_mate[pl.ds(j * q_rows, q_rows), :] = attend_rows(1 - x, j)
+    forward(OUT, 1)
+    for j in range(parts):
+        att[pl.ds(j * q_rows, q_rows), att_half] = attend_rows(x, j)
+        if j == 0:
+            att_swap.start()
+            forward(OUT, 2)
+    for d in range(3, nz):
+        forward(OUT, d)
+    for d in range(nz):
+        move(ACROSS, OUT, 2 * d + 1 - x).wait_recv()
+    att_swap.wait_recv()
 
     def product(block):
         return jnp.dot(att[...], wo_all[block], preferred_element_type=jnp.float32)
@@ -337,22 +420,27 @@
         store(which).wait()
 
     for kind in range(4):
-        for d in range(nz):
-            @pl.when(z - d >= 0)
-            def _():
-                pl.when(has_up)(lambda: move(UP, kind, s - 2 * d).wait_send())
-                move(ACROSS, kind, s - 2 * d).wait_send()
-
-            @pl.when(z + d < nz)
-            def _():
-                pl.when(has_down)(lambda: move(DOWN, kind, s + 2 * d).wait_send())
-                if d:
-                    move(ACROSS, kind, s + 2 * d).wait_send()
-    @pl.when(has_next)
+        if kind != OUT:
+            move(ACROSS, kind, s).wait_send()
+        for start in columns(kind):
+            for d in range(nz):
+                @pl.when(z - d >= 0)
+                def _():
+                    pl.when(has_up)(lambda: move(UP, kind, start - 2 * d).wait_send())
+                    if kind == OUT:
+                        move(ACROSS, kind, start - 2 * d).wait_send()
+
+                @pl.when(z + d < nz)
+                def _():
+                    pl.when(has_down)(lambda: move(DOWN, kind, start + 2 * d).wait_send())
+                    if kind == OUT and d:
+                        move(ACROSS, kind, start + 2 * d).wait_send()
+
+    @pl.when(has_up)
     def _():
         for i in range(3):
             halo(i).wait_send()
-    for one in (*part_moves, hop, to_y, to_core, pass_on):
+    for one in (x_swap, row_swap, col_swap, att_swap, *part_moves, hop, to_y, to_core, pass_on):
         one.wait_send()
 
 
@@ -383,26 +471,35 @@
     return pl.pallas_call(
         functools.partial(layer_kernel, n_sp, n_tp),
         out_shape=jax.ShapeDtypeStruct((rows, width), bf),
-        in_specs=[vmem] * 5 + [hbm] * 4,
+        in_specs=[vmem] * 4 + [hbm] * 5,
         out_specs=hbm,
         scratch_shapes=[
-            pltpu.VMEM((3, n_sp * depth, cols), bf),
+            pltpu.VMEM((3, n_sp * depth, cols // 2), bf),
+            pltpu.VMEM((3, depth, cols // 2), bf),
             pltpu.VMEM((n_sp, cols, out_cols), bf),
             pltpu.VMEM((rows, width), bf),
-            pltpu.VMEM((heads, 2 * SEG, (LEFT + 2) * SEG), f32),
+            pltpu.VMEM((rows, width), bf),
+            pltpu.VMEM((2 * rows, width), bf),
+            pltpu.VMEM((heads // 2, 2 * SEG, (LEFT + 2) * SEG), f32),
+            pltpu.VMEM((2 * rows, cols // 2), bf),
+            pltpu.VMEM((3 * rows, cols // 2), bf),
+            pltpu.VMEM((3 * rows, cols // 2), bf),
+            pltpu.VMEM((8, 3 * rows), jnp.int32),
+            pltpu.VMEM((2 * rows, 128), jnp.int32),
             pltpu.VMEM((rows, cols), bf),
-            pltpu.VMEM((2 * rows, cols), bf),
-            pltpu.VMEM((2 * rows, cols), bf),
-            pltpu.VMEM((8, 2 * rows), jnp.int32),
-            pltpu.VMEM((rows, cols), bf),
+            pltpu.VMEM((rows, cols // 2), bf),
             pltpu.VMEM((2, rows, chunk), bf),
             pltpu.VMEM((2, rows, chunk), bf),
             pltpu.VMEM((rows, chunk), bf),
             pltpu.VMEM((rows, chunk), bf),
             pltpu.VMEM((n_tp, rows, chunk), bf),
             dma((4,)),
+            dma((3,)),
+            dma(()),
             dma((3, 4, n_sp)),
             dma((4, n_sp)),
+            dma((4,)),
+            dma((4,)),
             dma((3,)),
             dma((3,)),
             dma((6,)),
@@ -410,13 +507,13 @@
             dma((n_tp,)),
         ],
         compiler_params=pltpu.CompilerParams(
-            collective_id=0, has_side_effects=True, vmem_limit_bytes=48 * 1024 * 1024
+            collective_id=0, has_side_effects=True, vmem_limit_bytes=60 * 1024 * 1024
         ),
-    )(tokens, doc_col, doc_row, norm_gain, line, w_key[0], w_value[0], w_query[0], w_out[0])
+    )(doc_col, doc_row, norm_gain, line, tokens, w_key[0], w_value[0], w_query[0], w_out[0])
 
 
 def fits_one(mesh):
-    return mesh.shape["sp"] % 2 == 0 and mesh.shape["sp"] <= 8 and mesh.shape["tp"] == 4
+    return mesh.shape["sp"] % 2 == 0 and 6 <= mesh.shape["sp"] <= 8 and mesh.shape["tp"] == 4
 
 
 def solution(mesh):

time: 141 us -> 113 us (0.80)
  the two profiles are of different devices: /device:TPU:3 before, /device:TPU:25 now
where the time goes in v2:
time: 113 us
  Pallas kernels  107 us (95%)
  local copies, waits for them, and re-layouts  5.57 us (5%)
    pallas_call x1, Pallas kernels, body_one(): pl.pallas_call(functools.partial(layer_kernel, n_sp, n_tp), out_shape=jax...  107 us
    unnamed x7, local copies, waits for them, and re-layouts  3.21 us

profile of v2, /device:TPU:25, one launch (start us, length us, event | category | flops | bytes accessed | tf_op | source)
XLA Modules:
  0.0 113.2 jit_solution(12474936799592309482)
XLA Ops:
  0.0 0.0 copy-start
  0.0 0.9 slice_reduce_fusion
  0.9 0.1 broadcast_in_dim.28
  0.9 0.0 copy-start.1
  0.9 0.1 broadcast_in_dim.13
  1.0 0.6 copy-done.1
  1.6 0.6 broadcast_in_dim.11.doc_row
  2.2 0.0 copy-done
  2.2 0.2 reverse
  2.4 0.1 slice.6
  2.5 0.7 pad_maximum_fusion.line_ref
  3.2 0.8 broadcast_in_dim.10.doc_col
  4.0 106.9 %shard_map.82 = bf16[256,2048]{1,0:T(8,128)(2,1)} custom-call(s32[256,128]{1,0:T(8,128)} %broadcast_in_dim.10.doc_col, s32[8,256]{1,0:T(8,128)} %broadcast_in_dim.11.doc_row, f32[1,2048]{1,0:T(1,128)} %gain_ref.1, f32[8,512]{1,0:T(8,128)} %pad_maximum_fusion.line_ref, bf16[256,2048]{1,0:T(8,128)(2,1)} %x_in.1, bf16[256,512]{1,0:T(8,128)(2,1)} %bitcast.7, ...), custom_call_target="tpu_custom_call" | custom-call | tf_op jit(solution)/shard_map/pallas_call | solution.py:471
  110.9 2.3 %copy.10 = bf16[256,2048]{1,0:T(8,128)(2,1)} copy(bf16[256,2048]{1,0:T(8,128)(2,1)} %shard_map.82) | data formatting | bytes 2097152
Async XLA Ops:
  0.0 2.2 %copy-start = (f32[1,8,257]{2,1,0:T(8,128)S(1)}, f32[1,8,257]{2,1,0:T(8,128)}, u32[]{:S(2)}) copy-start(f32[1,8,257]{2,1,0:T(8,128)} %param.15) | copy-start | bytes 24676
  0.9 0.7 copy-start.1

commit v3 on v2

--- a/solution.py
+++ b/solution.py
@@ -124,9 +124,8 @@
 
 def layer_kernel(
     n_sp, n_tp, doc_col, doc_row, gain_ref, line_ref, x_in, wk_in, wv_in, wq_in, wo_in, out_ref,
-    w_all, w_mate, wo_all, x_ref, x_mate, normed, bias, q_buf, k_all, v_all, docs_all, docs_col, att, att_mate,
-    part_out, part_in, hop_out, hop_in, done,
-    own_sem, mate_sem, x_sem, send_sem, recv_sem, swap_send, swap_recv, halo_send, halo_recv,
+    w_all, w_mate, wo_all, x_ref, x_mate, normed, bias, q_buf, k_all, v_all, docs_all, docs_col, att, att_mate, done,
+    own_sem, out_sem, mate_sem, x_sem, send_sem, recv_sem, swap_send, swap_recv, halo_send, halo_recv,
     tp_send, tp_recv, store_sem,
 ):
     rows, width = x_ref.shape
@@ -153,11 +152,10 @@
         return own_in[kind].at[:, pl.ds(pl.multiple_of(which * half_cols, half_cols), half_cols)]
 
     def own_copy(kind):
-        if kind == OUT:
-            src = wo_in.at[pl.ds(pl.multiple_of(t * cols, cols), cols), :]
-        else:
-            src = column_half(kind, x)
-        return pltpu.make_async_copy(src, slot(kind, s), own_sem.at[kind])
+        return pltpu.make_async_copy(column_half(kind, x), slot(kind, s), own_sem.at[kind])
+
+    def out_copy(r):
+        return pltpu.make_async_copy(wo_in.at[pl.ds(r * cols, cols), :], slot(OUT, 2 * r + x), out_sem.at[r])
 
     def mate_copy(kind):
         return pltpu.make_async_copy(column_half(kind, 1 - x), w_mate.at[kind], mate_sem.at[kind])
@@ -167,7 +165,12 @@
         own_copy(kind).start()
         mate_copy(kind).start()
     x_copy.start()
-    own_copy(OUT).start()
+
+    @pl.when(z == t)
+    def _():
+        for r in range(n_tp):
+            out_copy(r).start()
+
 
     def move(way, kind, block):
         target = (s + 2, s - 2, mate)[way]
@@ -204,7 +207,7 @@
     row_swap = swap(1, doc_row, docs_all.at[:, block_of(1 + x)])
     col_swap = swap(2, doc_col, docs_col.at[block_of(x), :])
     att_half = pl.ds(pl.multiple_of(x * half_cols, half_cols), half_cols)
-    att_swap = swap(3, att_mate, att.at[:, att_half])
+    att_swap = swap(3, att_mate, att.at[t, :, att_half])
 
     has_up, has_down = z < nz - 1, z > 0
 
@@ -222,8 +225,6 @@
     def send_own(kind):
         own_copy(kind).wait()
         along_z(kind, s)
-        if kind == OUT:
-            move(ACROSS, kind, s).start()
 
     def send_mate(kind):
         mate_copy(kind).wait()
@@ -233,26 +234,32 @@
         move(ACROSS, kind, mate).wait_recv()
         along_z(kind, mate)
 
-    def columns(kind):
-        return (s,) if kind == OUT else (s, mate)
-
     def forward(kind, d):
-        for start in columns(kind):
+        for start in (s, mate):
             @pl.when(z - d >= 0)
             def _():
                 block = start - 2 * d
                 move(UP, kind, block).wait_recv()
                 pl.when(has_up)(lambda: move(UP, kind, block).start())
-                if kind == OUT:
-                    move(ACROSS, kind, block).start()
 
             @pl.when(z + d < nz)
             def _():
                 block = start + 2 * d
                 move(DOWN, kind, block).wait_recv()
                 pl.when(has_down)(lambda: move(DOWN, kind, block).start())
-                if kind == OUT:
-                    move(ACROSS, kind, block).start()
+
+    sends_up, sends_down = (z >= t) & has_up, (z <= t) & has_down
+
+    def send_out(r):
+        pl.when(sends_up)(lambda: move(UP, OUT, 2 * r + x).start())
+        pl.when(sends_down)(lambda: move(DOWN, OUT, 2 * r + x).start())
+        move(ACROSS, OUT, 2 * r + x).start()
+
+    def forward_out(r):
+        @pl.when(z != t)
+        def _():
+            move(UP, OUT, 2 * r + x).wait_recv()
+            send_out(r)
 
     def normalize(src, which):
         wide = src[...].astype(jnp.float32)
@@ -301,11 +308,10 @@
         forward(KEY, d)
     send_own(QUERY)
     forward_mate(QUERY)
-    forward(VALUE, 1)
+    for d in range(1, nz):
+        forward(VALUE, d)
     x_swap.wait_recv()
     normalize(x_mate, 1 - x)
-    for d in range(2, nz):
-        forward(VALUE, d)
     k_all[pl.ds(rows, 2 * rows), :] = project(KEY).astype(jnp.bfloat16)
     row_swap.wait_recv()
     col_swap.wait_recv()
@@ -316,7 +322,13 @@
     for d in range(2, nz - 1):
         forward(QUERY, d)
     pl.when(has_up)(lambda: halo(1).start())
-    send_own(OUT)
+
+    @pl.when(z == t)
+    def _():
+        for r in range(n_tp):
+            out_copy(r).wait()
+            send_out(r)
+
     forward(QUERY, nz - 1)
     q_buf[...] = (project(QUERY).astype(jnp.bfloat16).astype(jnp.float32) * HEAD_DIM ** (-0.5)).astype(jnp.bfloat16)
 
@@ -352,50 +364,42 @@
             found.append(jnp.where(low, both[0], both[1]).astype(jnp.bfloat16))
         return jnp.concatenate(found, axis=1)
 
+    def tp_move(i, ref, which, target):
+        return pltpu.make_async_remote_copy(
+            src_ref=ref.at[which], dst_ref=ref.at[which], send_sem=tp_send.at[i], recv_sem=tp_recv.at[i],
+            device_id={"tp": target}, device_id_type=MESH,
+        )
+
+    att_y = tp_move(0, att, t, t_y)
+    att_core = tp_move(1, att, t, t_core)
+    att_on = tp_move(2, att, t_y, t_core)
+
     parts = rows // q_rows
     for j in range(parts):
         att_mate[pl.ds(j * q_rows, q_rows), :] = attend_rows(1 - x, j)
-    forward(OUT, 1)
+    forward_out(0)
     for j in range(parts):
-        att[pl.ds(j * q_rows, q_rows), att_half] = attend_rows(x, j)
+        att[t, pl.ds(j * q_rows, q_rows), att_half] = attend_rows(x, j)
         if j == 0:
             att_swap.start()
-            forward(OUT, 2)
-    for d in range(3, nz):
-        forward(OUT, d)
-    for d in range(nz):
-        move(ACROSS, OUT, 2 * d + 1 - x).wait_recv()
+    forward_out(1)
     att_swap.wait_recv()
-
-    def product(block):
-        return jnp.dot(att[...], wo_all[block], preferred_element_type=jnp.float32)
-
-    def chunk_product(which):
-        each = chunk // wo_in.shape[1]
-        return jnp.concatenate([product(which * each + i) for i in range(each)], axis=1)
-
-    def tp_move(i, src, dst, target):
-        return pltpu.make_async_remote_copy(
-            src_ref=src, dst_ref=dst, send_sem=tp_send.at[i], recv_sem=tp_recv.at[i],
-            device_id={"tp": target}, device_id_type=MESH,
-        )
-
-    part_moves = [tp_move(i, part_out.at[i], part_in.at[i], t_core) for i in range(2)]
+    att_y.start()
+    att_core.start()
+    for r in range(2, n_tp):
+        forward_out(r)
+    att_y.wait_recv()
+    att_on.start()
+    att_core.wait_recv()
+    att_on.wait_recv()
+    for r in range(n_tp):
+        move(ACROSS, OUT, 2 * r + 1 - x).wait_recv()
+    sums = [x_ref[:, pl.ds(pl.multiple_of(t * chunk + i * (chunk // 2), chunk // 2), chunk // 2)].astype(jnp.float32) for i in range(2)]
     for i in range(2):
-        other = (1 - ty if i == 0 else ty) * 2 + (1 - tc)
-        part_out[i] = chunk_product(other).astype(jnp.bfloat16)
-        part_moves[i].start()
-    far = chunk_product(t_y)
-    part_moves[0].wait_recv()
-    hop_out[...] = (far + part_in[0].astype(jnp.float32)).astype(jnp.bfloat16)
-    hop = tp_move(2, hop_out, hop_in, t_y)
-    hop.start()
-    near_sum = chunk_product(t)
-    part_moves[1].wait_recv()
-    near_sum = near_sum + part_in[1].astype(jnp.float32)
-    near_sum = near_sum + x_ref[:, pl.ds(pl.multiple_of(t * chunk, chunk), chunk)].astype(jnp.float32)
-    hop.wait_recv()
-    done[t] = (near_sum + hop_in[...].astype(jnp.float32)).astype(jnp.bfloat16)
+        made = jnp.zeros_like(sums[i])
+        for r in range(n_tp):
+            made = made + jnp.dot(att[r], wo_all[2 * r + i], preferred_element_type=jnp.float32)
+        done[t, :, pl.ds(i * (chunk // 2), chunk // 2)] = (sums[i] + made).astype(jnp.bfloat16)
 
     def store(which):
         return pltpu.make_async_copy(
@@ -403,9 +407,9 @@
         )
 
     far_core = (1 - ty) * 2 + (1 - tc)
-    to_y = tp_move(3, done.at[t], done.at[t], t_y)
-    to_core = tp_move(4, done.at[t], done.at[t], t_core)
-    pass_on = tp_move(5, done.at[t_y], done.at[t_y], t_core)
+    to_y = tp_move(3, done, t, t_y)
+    to_core = tp_move(4, done, t, t_core)
+    pass_on = tp_move(5, done, t_y, t_core)
     to_y.start()
     to_core.start()
     store(t).start()
@@ -419,28 +423,27 @@
     for which in range(n_tp):
         store(which).wait()
 
-    for kind in range(4):
-        if kind != OUT:
-            move(ACROSS, kind, s).wait_send()
-        for start in columns(kind):
+    for kind in range(3):
+        move(ACROSS, kind, s).wait_send()
+        for start in (s, mate):
             for d in range(nz):
                 @pl.when(z - d >= 0)
                 def _():
                     pl.when(has_up)(lambda: move(UP, kind, start - 2 * d).wait_send())
-                    if kind == OUT:
-                        move(ACROSS, kind, start - 2 * d).wait_send()
 
                 @pl.when(z + d < nz)
                 def _():
                     pl.when(has_down)(lambda: move(DOWN, kind, start + 2 * d).wait_send())
-                    if kind == OUT and d:
-                        move(ACROSS, kind, start + 2 * d).wait_send()
+    for r in range(n_tp):
+        pl.when(sends_up)(lambda: move(UP, OUT, 2 * r + x).wait_send())
+        pl.when(sends_down)(lambda: move(DOWN, OUT, 2 * r + x).wait_send())
+        move(ACROSS, OUT, 2 * r + x).wait_send()
 
     @pl.when(has_up)
     def _():
         for i in range(3):
             halo(i).wait_send()
-    for one in (x_swap, row_swap, col_swap, att_swap, *part_moves, hop, to_y, to_core, pass_on):
+    for one in (x_swap, row_swap, col_swap, att_swap, att_y, att_core, att_on, to_y, to_core, pass_on):
         one.wait_send()
 
 
@@ -486,14 +489,11 @@
             pltpu.VMEM((3 * rows, cols // 2), bf),
             pltpu.VMEM((8, 3 * rows), jnp.int32),
             pltpu.VMEM((2 * rows, 128), jnp.int32),
-            pltpu.VMEM((rows, cols), bf),
+            pltpu.VMEM((n_tp, rows, cols), bf),
             pltpu.VMEM((rows, cols // 2), bf),
-            pltpu.VMEM((2, rows, chunk), bf),
-            pltpu.VMEM((2, rows, chunk), bf),
-            pltpu.VMEM((rows, chunk), bf),
-            pltpu.VMEM((rows, chunk), bf),
             pltpu.VMEM((n_tp, rows, chunk), bf),
-            dma((4,)),
+            dma((3,)),
+            dma((n_tp,)),
             dma((3,)),
             dma(()),
             dma((3, 4, n_sp)),
@@ -513,7 +513,7 @@
 
 
 def fits_one(mesh):
-    return mesh.shape["sp"] % 2 == 0 and 6 <= mesh.shape["sp"] <= 8 and mesh.shape["tp"] == 4
+    return mesh.shape["tp"] == 4 and mesh.shape["sp"] == 2 * mesh.shape["tp"]
 
 
 def solution(mesh):

time: 113 us -> 109 us (0.965)
  the two profiles are of different devices: /device:TPU:25 before, /device:TPU:0 now
where the time goes in v3:
time: 109 us
  Pallas kernels  103 us (94%)
  local copies, waits for them, and re-layouts  5.57 us (5%)
    pallas_call x1, Pallas kernels, body_one(): pl.pallas_call(functools.partial(layer_kernel, n_sp, n_tp), out_shape=jax...  103 us
    unnamed x7, local copies, waits for them, and re-layouts  3.21 us

profile of v3, /device:TPU:0, one launch (start us, length us, event | category | flops | bytes accessed | tf_op | source)
XLA Modules:
  0.0 109.1 jit_solution(17753866843530289334)
XLA Ops:
  0.0 0.0 copy-start
  0.0 0.9 slice_reduce_fusion
  0.9 0.1 broadcast_in_dim.28
  0.9 0.0 copy-start.1
  0.9 0.1 broadcast_in_dim.13
  1.0 0.6 copy-done.1
  1.6 0.6 broadcast_in_dim.11.doc_row
  2.2 0.0 copy-done
  2.2 0.2 reverse
  2.4 0.1 slice.6
  2.5 0.7 pad_maximum_fusion.line_ref
  3.2 0.8 broadcast_in_dim.10.doc_col
  4.0 102.8 %shard_map.82 = bf16[256,2048]{1,0:T(8,128)(2,1)} custom-call(s32[256,128]{1,0:T(8,128)} %broadcast_in_dim.10.doc_col, s32[8,256]{1,0:T(8,128)} %broadcast_in_dim.11.doc_row, f32[1,2048]{1,0:T(1,128)} %gain_ref.1, f32[8,512]{1,0:T(8,128)} %pad_maximum_fusion.line_ref, bf16[256,2048]{1,0:T(8,128)(2,1)} %x_in.1, bf16[256,512]{1,0:T(8,128)(2,1)} %bitcast.7, ...), custom_call_target="tpu_custom_call" | custom-call | tf_op jit(solution)/shard_map/pallas_call | solution.py:474
  106.8 2.3 %copy.10 = bf16[256,2048]{1,0:T(8,128)(2,1)} copy(bf16[256,2048]{1,0:T(8,128)(2,1)} %shard_map.82) | data formatting | bytes 2097152
Async XLA Ops:
  0.0 2.2 %copy-start = (f32[1,8,257]{2,1,0:T(8,128)S(1)}, f32[1,8,257]{2,1,0:T(8,128)}, u32[]{:S(2)}) copy-start(f32[1,8,257]{2,1,0:T(8,128)} %param.15) | copy-start | bytes 24676
  0.9 0.7 copy-start.1
